TPU v7x, 128 devices: a whole 4x4x4 slice. The times are simulated.
128 devices in a mesh: kv: 16 (over z, y), tp: 8 (over x, core).
Axes of the slice: x: 4, y: 4, z: 4, core: 2. Of those that a mesh axis runs over, the one named last changes fastest.
Arguments:
- block_in: bfloat16 [128, 4096], P(None, ('kv', 'tp')), may hold values from -30 to 30
- before_gain: bfloat16 [4096], P('kv'), may hold values from 0.099609375 to 1.8984375
- before_gate: bfloat16 [4096, 11264], P('kv', 'tp'), may hold values from -0.09375 to 0.09375
- before_up: bfloat16 [4096, 11264], P('kv', 'tp'), may hold values from -0.09375 to 0.09375
- before_down: bfloat16 [11264, 4096], P('tp', 'kv'), may hold values from -0.0546875 to 0.0546875
- mix_gain: bfloat16 [4096], P('kv'), may hold values from 0.099609375 to 1.8984375
- input_gate: bfloat16 [4096, 8192], P('kv', 'tp'), may hold values from -0.09375 to 0.09375
- input_value: bfloat16 [4096, 8192], P('kv', 'tp'), may hold values from -0.09375 to 0.09375
- input_write: bfloat16 [4096, 2048], P('kv', 'tp'), may hold values from -0.09375 to 0.09375
- input_read: bfloat16 [4096, 2048], P('kv', 'tp'), may hold values from -0.09375 to 0.09375
- input_step: bfloat16 [4096, 128], P('kv', 'tp'), may hold values from -0.09375 to 0.09375
- step_bias: float32 [128], P('tp'), may hold values from -3 to 0
- decay_log: float32 [128], P('tp'), may hold values from -1 to 1.4
- skip_gain: float32 [128], P('tp'), may hold values from 0.5 to 2
- value_taps: bfloat16 [4, 8192], P(None, 'tp'), may hold values from -3 to 3
- write_taps: bfloat16 [4, 2048], P(None, 'tp'), may hold values from -3 to 3
- read_taps: bfloat16 [4, 2048], P(None, 'tp'), may hold values from -3 to 3
- value_window: bfloat16 [128, 3, 8192], P('kv', None, 'tp'), may hold values from -6 to 6
- write_window: bfloat16 [128, 3, 2048], P('kv', None, 'tp'), may hold values from -6 to 6
- read_window: bfloat16 [128, 3, 2048], P('kv', None, 'tp'), may hold values from -6 to 6
- scan_state: float32 [128, 128, 64, 128], P('kv', 'tp'), may hold values from -2 to 2
- group_gain: bfloat16 [8192], P('tp'), may hold values from 0.099609375 to 1.8984375
- mixer_out: bfloat16 [8192, 4096], P('tp', 'kv'), may hold values from -0.0625 to 0.0625
- after_gain: bfloat16 [4096], P('kv'), may hold values from 0.099609375 to 1.8984375
- after_gate: bfloat16 [4096, 11264], P('kv', 'tp'), may hold values from -0.09375 to 0.09375
- after_up: bfloat16 [4096, 11264], P('kv', 'tp'), may hold values from -0.09375 to 0.09375
- after_down: bfloat16 [11264, 4096], P('tp', 'kv'), may hold values from -0.0546875 to 0.0546875
Outputs:
- block_out: bfloat16 [128, 4096], P(None, ('kv', 'tp'))
- state_next: float32 [128, 128, 64, 128], P('kv', 'tp')
- value_next: bfloat16 [128, 3, 8192], P('kv', None, 'tp')
- write_next: bfloat16 [128, 3, 2048], P('kv', None, 'tp')
- read_next: bfloat16 [128, 3, 2048], P('kv', None, 'tp')
All inputs are finite; a program needn't handle non-finite values.
Results may differ from a plain program's by a relative error of at most 0.0085.
Values may be sent and summed in bfloat16 or wider, within the bound.
A program may use at most 64 MiB of HBM per device.

v0:
```python
import jax
import jax.numpy as jnp
from jax import lax
from jax.sharding import PartitionSpec as P

D = 4096
HEAD_DIM = 64
STATE = 128
EPS = 1e-06


def copy_for_each(shard, axis):
    copies = jnp.broadcast_to(shard, (lax.axis_size(axis), *shard.shape))
    return lax.all_to_all(copies, axis, split_axis=0, concat_axis=0, tiled=True)


def in_order(blocks, dim):
    shape = list(blocks.shape[1:])
    shape[dim] *= blocks.shape[0]
    return jnp.moveaxis(blocks, 0, dim).reshape(shape)


def gather_directly(shard, axis, dim):
    blocks = copy_for_each(shard, axis)
    return in_order(blocks, dim)


def in_blocks(shard, dim, length):
    before, after = (shard.shape[:dim], shard.shape[dim + 1 :])
    return jnp.moveaxis(shard.reshape(*before, length, -1, *after), dim, 0)


def sent_and_summed(shard, axis, dim):
    length = lax.axis_size(axis)
    blocks = lax.all_to_all(in_blocks(shard, dim, length), axis, 0, 0, tiled=True)
    return jnp.sum(blocks, axis=0)


def sum_at_owner(shard, axis, dim):
    blocks = in_blocks(shard, dim, lax.axis_size(axis))
    arrived = lax.all_to_all(blocks, axis, split_axis=0, concat_axis=0, tiled=True)
    return arrived.astype(jnp.float32).sum(axis=0)


def side_by_side(arrays, axis, dim, along):
    ends, at = ([], 0)
    for a in arrays[:-1]:
        at += a.shape[along]
        ends.append(at)
    both = jnp.concatenate(arrays, axis=along)
    return tuple(jnp.split(sum_at_owner(both, axis, dim), ends, axis=along))


def in_one_piece(arrays, axis, dim, along):
    columns = [a.reshape(*a.shape[:along], -1) for a in arrays]
    both = jnp.concatenate(columns, axis=along)
    result, at, gathered = (sent_and_summed(both, axis, dim), 0, [])
    for a, column in zip(arrays, columns):
        share = result[..., at : at + column.shape[along]]
        gathered.append(share.reshape(*share.shape[:along], *a.shape[along:]))
        at += column.shape[along]
    return tuple(gathered)


def lifted_rows(current, gain_vec):
    gathered = gather_directly(current, "tp", 1)
    widened = gathered.astype(jnp.float32)
    squares = jnp.sum(widened * widened, axis=1)
    lifted = (widened * gain_vec.astype(jnp.float32)[None, :]).astype(jnp.bfloat16)
    return (lifted, squares)


def column_sums(partial_terms):
    return sent_and_summed(partial_terms, "tp", 1)


def half_channel(current, gain_vec, gate_weight, up_weight, down_weight):
    lifted, squares = lifted_rows(current, gain_vec)
    gate_part = jnp.dot(lifted, gate_weight, preferred_element_type=jnp.float32)
    up_part = jnp.dot(lifted, up_weight, preferred_element_type=jnp.float32)
    spread_squares = jnp.broadcast_to(squares[:, None], (squares.shape[0], lax.axis_size("kv")))
    gate_sum, up_sum, totals = (
        *side_by_side((gate_part.astype(jnp.bfloat16), up_part.astype(jnp.bfloat16)), "kv", 1, 0),
        sum_at_owner(spread_squares.astype(jnp.bfloat16), "kv", 1),
    )
    row_scale = lax.rsqrt(totals / D + EPS)
    hidden_share = (jax.nn.silu(gate_sum * row_scale) * (up_sum * row_scale)).astype(jnp.bfloat16)
    down_sum = jnp.dot(
        gather_directly(hidden_share, "kv", 1), down_weight, preferred_element_type=jnp.float32
    )
    returned = column_sums(down_sum)
    return (current.astype(jnp.float32) + 0.5 * returned).astype(jnp.bfloat16)


def short_conv(window_state, fresh, taps):
    window = jnp.concatenate([window_state, fresh[:, None, :]], axis=1)
    conv_sum = jnp.sum(window.astype(jnp.float32) * taps.astype(jnp.float32)[None], axis=1)
    return (jax.nn.silu(conv_sum), window[:, 1:])


def spread_groups(vectors, heads):
    count = vectors.shape[0]
    groups = vectors.shape[1] // STATE
    shaped = vectors.reshape(count, groups, 1, STATE)
    return jnp.broadcast_to(shaped, (count, groups, heads // groups, STATE)).reshape(
        count, heads, STATE
    )


def state_update(
    gate_rows,
    value_conv,
    write_conv,
    read_conv,
    step_raw,
    step_bias,
    decay_log,
    skip_gain,
    scan_state,
):
    count = value_conv.shape[0]
    heads = step_bias.shape[0]
    step_size = jax.nn.softplus(step_raw + step_bias[None, :])
    decay = jnp.exp(-step_size * jnp.exp(decay_log)[None, :])
    value_heads = value_conv.reshape(count, heads, HEAD_DIM)
    write_heads = spread_groups(write_conv, heads)
    read_heads = spread_groups(read_conv, heads)
    state_next = (
        decay[:, :, None, None] * scan_state
        + (step_size[:, :, None] * value_heads)[:, :, :, None] * write_heads[:, :, None, :]
    )
    readout = (
        jnp.sum(state_next * read_heads[:, :, None, :], axis=3)
        + skip_gain[None, :, None] * value_heads
    )
    gated = readout.reshape(count, heads * HEAD_DIM) * jax.nn.silu(gate_rows.astype(jnp.float32))
    groups = write_conv.shape[1] // STATE
    grouped = gated.reshape(count, groups, heads * HEAD_DIM // groups)
    grouped = grouped * lax.rsqrt(jnp.mean(grouped * grouped, axis=2, keepdims=True) + EPS)
    return (grouped.reshape(count, heads * HEAD_DIM), state_next)


def local(
    block_in,
    before_gain,
    before_gate,
    before_up,
    before_down,
    mix_gain,
    input_gate,
    input_value,
    input_write,
    input_read,
    input_step,
    step_bias,
    decay_log,
    skip_gain,
    value_taps,
    write_taps,
    read_taps,
    value_window,
    write_window,
    read_window,
    scan_state,
    group_gain,
    mixer_out,
    after_gain,
    after_gate,
    after_up,
    after_down,
):
    first_out = half_channel(block_in, before_gain, before_gate, before_up, before_down)
    lifted, squares = lifted_rows(first_out, mix_gain)
    gate_part = jnp.dot(lifted, input_gate, preferred_element_type=jnp.float32)
    value_part = jnp.dot(lifted, input_value, preferred_element_type=jnp.float32)
    write_part = jnp.dot(lifted, input_write, preferred_element_type=jnp.float32)
    read_part = jnp.dot(lifted, input_read, preferred_element_type=jnp.float32)
    step_part = jnp.dot(lifted, input_step, preferred_element_type=jnp.float32)
    gate_sum, value_sum, write_sum, read_sum, step_sum, totals = in_one_piece(
        (gate_part, value_part, write_part, read_part, step_part, squares), "kv", 0, 1
    )
    mix_scale = lax.rsqrt(totals / D + EPS)[:, None]
    gate_rows = (gate_sum * mix_scale).astype(jnp.bfloat16)
    value_fresh = (value_sum * mix_scale).astype(jnp.bfloat16)
    write_fresh = (write_sum * mix_scale).astype(jnp.bfloat16)
    read_fresh = (read_sum * mix_scale).astype(jnp.bfloat16)
    step_raw = step_sum * mix_scale
    value_conv, value_next = short_conv(value_window, value_fresh, value_taps)
    write_conv, write_next = short_conv(write_window, write_fresh, write_taps)
    read_conv, read_next = short_conv(read_window, read_fresh, read_taps)
    normed, state_next = state_update(
        gate_rows,
        value_conv,
        write_conv,
        read_conv,
        step_raw,
        step_bias,
        decay_log,
        skip_gain,
        scan_state,
    )
    mixer_rows = (normed * group_gain.astype(jnp.float32)[None, :]).astype(jnp.bfloat16)
    back_part = jnp.dot(
        lax.all_gather(mixer_rows, "kv", axis=0, tiled=True),
        mixer_out,
        preferred_element_type=jnp.float32,
    )
    returned = column_sums(back_part)
    middle = (first_out.astype(jnp.float32) + returned).astype(jnp.bfloat16)
    block_out = half_channel(middle, after_gain, after_gate, after_up, after_down)
    return (block_out, state_next, value_next, write_next, read_next)


def solution(mesh):
    placed = (
        P(None, ("kv", "tp")),
        P("kv"),
        P("kv", "tp"),
        P("kv", "tp"),
        P("tp", "kv"),
        P("kv"),
        P("kv", "tp"),
        P("kv", "tp"),
        P("kv", "tp"),
        P("kv", "tp"),
        P("kv", "tp"),
        P("tp"),
        P("tp"),
        P("tp"),
        P(None, "tp"),
        P(None, "tp"),
        P(None, "tp"),
        P("kv", None, "tp"),
        P("kv", None, "tp"),
        P("kv", None, "tp"),
        P("kv", "tp", None, None),
        P("tp"),
        P("tp", "kv"),
        P("kv"),
        P("kv", "tp"),
        P("kv", "tp"),
        P("tp", "kv"),
    )
    return jax.shard_map(
        local,
        mesh=mesh,
        in_specs=placed,
        out_specs=(
            P(None, ("kv", "tp")),
            P("kv", "tp", None, None),
            P("kv", None, "tp"),
            P("kv", None, "tp"),
            P("kv", None, "tp"),
        ),
        check_vma=False,
    )
```

profile of v0, /device:TPU:1, one launch (start us, length us, event | category | flops | bytes accessed | tf_op | source)
XLA Modules:
  0.0 210.5 jit_solution(9722446378386201120)
XLA Ops:
  0.6 1.4 broadcast_in_dim.20
  2.1 5.8 %all-to-all-start = ((bf16[8,128,32]{1,2,0:T(8,128)(2,1)}), bf16[8,128,32]{1,2,0:T(8,128)(2,1)S(1)}, u32[]{:S(2)}, u32[]{:S(2)}) async-start(bf16[8,128,32]{1,2,0:T(8,128)(2,1)} %broadcast_in_dim.20), calls=%async_computation | async-start | bytes 131072 | tf_op jit(solution)/shard_map/all_to_all | solution.py:14
  7.8 0.7 convert_element_type.166
  8.5 4.2 %all-to-all-done = bf16[8,128,32]{1,2,0:T(8,128)(2,1)S(1)} async-done(((bf16[8,128,32]{1,2,0:T(8,128)(2,1)}), bf16[8,128,32]{1,2,0:T(8,128)(2,1)S(1)}, u32[]{:S(2)}, u32[]{:S(2)}) %all-to-all-start) | async-done | bytes 65568 | tf_op jit(solution)/shard_map/all_to_all | solution.py:14
  12.7 0.1 fusion.6
  12.8 0.3 convolution_convert_fusion.2
  13.1 1.4 convolution_convert_fusion.3
  14.6 0.6 transpose.92
  15.2 7.8 %all-to-all-start.2 = ((bf16[16,128,1]{1,2,0:T(2,128)(2,1)}), bf16[16,128,1]{1,2,0:T(2,128)(2,1)S(1)}, u32[]{:S(2)}, u32[]{:S(2)}) async-start(bf16[16,128,1]{1,2,0:T(2,128)(2,1)} %transpose.92), calls=%async_computation.2 | async-start | bytes 16384 | tf_op jit(solution)/shard_map/all_to_all | solution.py:41
  23.1 1.1 copy.47
  24.2 5.1 %all-to-all-done.2 = bf16[16,128,1]{1,2,0:T(2,128)(2,1)S(1)} async-done(((bf16[16,128,1]{1,2,0:T(2,128)(2,1)}), bf16[16,128,1]{1,2,0:T(2,128)(2,1)S(1)}, u32[]{:S(2)}, u32[]{:S(2)}) %all-to-all-start.2) | async-done | bytes 4128 | tf_op jit(solution)/shard_map/all_to_all | solution.py:41
  29.3 3.7 %all-to-all-start.1 = ((bf16[16,256,88]{1,2,0:T(8,128)(2,1)}), bf16[16,256,88]{1,2,0:T(8,128)(2,1)S(1)}, u32[]{:S(2)}, u32[]{:S(2)}) async-start(bf16[16,256,88]{1,2,0:T(8,128)(2,1)} %bitcast.3), calls=%async_computation.1 | async-start | bytes 1441792 | tf_op jit(solution)/shard_map/all_to_all | solution.py:41
  33.1 11.6 %all-to-all-done.1 = bf16[16,256,88]{1,2,0:T(8,128)(2,1)S(1)} async-done(((bf16[16,256,88]{1,2,0:T(8,128)(2,1)}), bf16[16,256,88]{1,2,0:T(8,128)(2,1)S(1)}, u32[]{:S(2)}, u32[]{:S(2)}) %all-to-all-start.1) | async-done | bytes 720928 | tf_op jit(solution)/shard_map/all_to_all | solution.py:41
  44.7 0.1 convert_reduce_fusion.1
  44.9 0.8 broadcast_in_dim.21
  45.6 4.3 %all-to-all-start.3 = ((bf16[16,128,88]{1,2,0:T(8,128)(2,1)}), bf16[16,128,88]{1,2,0:T(8,128)(2,1)}, u32[]{:S(2)}, u32[]{:S(2)}) async-start(bf16[16,128,88]{1,2,0:T(8,128)(2,1)} %broadcast_in_dim.21), calls=%async_computation.3 | async-start | bytes 720896 | tf_op jit(solution)/shard_map/all_to_all | solution.py:14
  50.0 0.3 copy.48
  50.4 7.8 %all-to-all-done.3 = bf16[16,128,88]{1,2,0:T(8,128)(2,1)} async-done(((bf16[16,128,88]{1,2,0:T(8,128)(2,1)}), bf16[16,128,88]{1,2,0:T(8,128)(2,1)}, u32[]{:S(2)}, u32[]{:S(2)}) %all-to-all-start.3) | async-done | bytes 360480 | tf_op jit(solution)/shard_map/all_to_all | solution.py:14
  58.1 1.3 convolution_bitcast_fusion.1
  59.5 11.7 %all_to_all.65 = f32[8,128,32]{1,2,0:T(8,128)S(1)} all-to-all(f32[8,128,32]{1,2,0:T(8,128)S(1)} %convolution_bitcast_fusion.1), channel_id=1, replica_groups=mesh['kv'=16,'tp'=8] {'tp'}, dimensions={0} | all-to-all | bytes 262144 | tf_op jit(solution)/shard_map/all_to_all | solution.py:35
  71.2 0.6 broadcast_in_dim.22
  71.8 4.1 %all-to-all-start.5 = ((bf16[8,128,32]{1,2,0:T(8,128)(2,1)}), bf16[8,128,32]{1,2,0:T(8,128)(2,1)S(1)}, u32[]{:S(2)}, u32[]{:S(2)}) async-start(bf16[8,128,32]{1,2,0:T(8,128)(2,1)} %broadcast_in_dim.22), calls=%async_computation.5 | async-start | bytes 131072 | tf_op jit(solution)/shard_map/all_to_all | solution.py:14
  76.0 4.9 %all-to-all-done.5 = bf16[8,128,32]{1,2,0:T(8,128)(2,1)S(1)} async-done(((bf16[8,128,32]{1,2,0:T(8,128)(2,1)}), bf16[8,128,32]{1,2,0:T(8,128)(2,1)S(1)}, u32[]{:S(2)}, u32[]{:S(2)}) %all-to-all-start.5) | async-done | bytes 65568 | tf_op jit(solution)/shard_map/all_to_all | solution.py:14
  80.8 0.2 copy.50
  81.1 0.2 reshape.176
  81.4 0.2 fusion
  81.6 0.2 fusion.2
  81.9 0.2 fusion.7
  82.1 0.2 fusion.9
  82.3 0.1 fusion.27
  82.5 0.2 concatenate.28
  82.7 1.3 concatenate.23
  83.9 3.7 %all-to-all-start.6 = ((f32[16,8,2577]{2,1,0:T(8,128)}), f32[16,8,2577]{2,1,0:T(8,128)S(1)}, u32[]{:S(2)}, u32[]{:S(2)}) async-start(f32[16,8,2577]{2,1,0:T(8,128)} %concatenate.23), calls=%async_computation.6 | async-start | bytes 2752512 | tf_op jit(solution)/shard_map/all_to_all | solution.py:35
  87.9 20.5 %all-to-all-done.6 = f32[16,8,2577]{2,1,0:T(8,128)S(1)} async-done(((f32[16,8,2577]{2,1,0:T(8,128)}), f32[16,8,2577]{2,1,0:T(8,128)S(1)}, u32[]{:S(2)}, u32[]{:S(2)}) %all-to-all-start.6) | async-done | bytes 1319456 | tf_op jit(solution)/shard_map/all_to_all | solution.py:35
  108.5 0.2 fusion.33
  109.2 0.1 multiply_multiply_fusion
  109.3 5.3 %multiply_reduce_fusion = (f32[8,16,64]{2,1,0:T(8,128)S(1)}, f32[8,16,64,128]{3,2,1,0:T(8,128)}) fusion(f32[8,16,128]{2,1,0:T(8,128)S(1)} %broadcast_bitcast_fusion, f32[8,16,128]{2,1,0:T(8,128)S(1)} %broadcast_bitcast_fusion.1, f32[8,16,64]{2,1,0:T(8,128)S(1)} %multiply_multiply_fusion, f32[8,16,64,128]{3,2,1,0:T(8,128)} %param.47, ...), kind=kLoop, calls=%fused_computation | loop fusion | flops 5234688 | bytes 8585728 | tf_op jit(solution)/shard_map/reduce_sum | solution.py:133
  114.8 0.1 reduce_sum.166
  114.9 16.0 %all_gather.3 = bf16[128,1024]{1,0:T(8,128)(2,1)S(1)} all-gather(bf16[8,1024]{1,0:T(8,128)(2,1)S(1)} %multiply_convert_fusion.1), channel_id=1, replica_groups=mesh['kv'=16,'tp'=8] {'kv'}, dimensions={0}, use_global_device_ids=true | all-gather | bytes 278528 | tf_op jit(solution)/shard_map/all_gather | solution.py:204
  130.9 0.3 fusion.37
  131.3 15.1 %all_to_all.66 = f32[8,128,32]{1,2,0:T(8,128)S(1)} all-to-all(f32[8,128,32]{1,2,0:T(8,128)S(1)} %bitcast.91), channel_id=1, replica_groups=mesh['kv'=16,'tp'=8] {'tp'}, dimensions={0} | all-to-all | bytes 262144 | tf_op jit(solution)/shard_map/all_to_all | solution.py:35
  146.4 0.6 broadcast_in_dim.28
  147.1 4.1 %all-to-all-start.8 = ((bf16[8,128,32]{1,2,0:T(8,128)(2,1)}), bf16[8,128,32]{1,2,0:T(8,128)(2,1)S(1)}, u32[]{:S(2)}, u32[]{:S(2)}) async-start(bf16[8,128,32]{1,2,0:T(8,128)(2,1)} %broadcast_in_dim.28), calls=%async_computation.8 | async-start | bytes 131072 | tf_op jit(solution)/shard_map/all_to_all | solution.py:14
  151.2 4.9 %all-to-all-done.8 = bf16[8,128,32]{1,2,0:T(8,128)(2,1)S(1)} async-done(((bf16[8,128,32]{1,2,0:T(8,128)(2,1)}), bf16[8,128,32]{1,2,0:T(8,128)(2,1)S(1)}, u32[]{:S(2)}, u32[]{:S(2)}) %all-to-all-start.8) | async-done | bytes 65568 | tf_op jit(solution)/shard_map/all_to_all | solution.py:14
  156.0 0.1 fusion.5
  156.2 0.3 convolution_convert_fusion
  156.5 0.3 convolution_convert_fusion.1
  156.8 0.6 transpose.97
  157.4 4.7 %all-to-all-start.10 = ((bf16[16,128,1]{1,2,0:T(2,128)(2,1)}), bf16[16,128,1]{1,2,0:T(2,128)(2,1)S(1)}, u32[]{:S(2)}, u32[]{:S(2)}) async-start(bf16[16,128,1]{1,2,0:T(2,128)(2,1)} %transpose.97), calls=%async_computation.10 | async-start | bytes 16384 | tf_op jit(solution)/shard_map/all_to_all | solution.py:41
  162.2 1.1 copy.53
  163.4 5.2 %all-to-all-done.10 = bf16[16,128,1]{1,2,0:T(2,128)(2,1)S(1)} async-done(((bf16[16,128,1]{1,2,0:T(2,128)(2,1)}), bf16[16,128,1]{1,2,0:T(2,128)(2,1)S(1)}, u32[]{:S(2)}, u32[]{:S(2)}) %all-to-all-start.10) | async-done | bytes 4128 | tf_op jit(solution)/shard_map/all_to_all | solution.py:41
  168.5 3.6 %all-to-all-start.9 = ((bf16[16,256,88]{1,2,0:T(8,128)(2,1)}), bf16[16,256,88]{1,2,0:T(8,128)(2,1)S(1)}, u32[]{:S(2)}, u32[]{:S(2)}) async-start(bf16[16,256,88]{1,2,0:T(8,128)(2,1)} %bitcast.28), calls=%async_computation.9 | async-start | bytes 1441792 | tf_op jit(solution)/shard_map/all_to_all | solution.py:41
  172.2 11.6 %all-to-all-done.9 = bf16[16,256,88]{1,2,0:T(8,128)(2,1)S(1)} async-done(((bf16[16,256,88]{1,2,0:T(8,128)(2,1)}), bf16[16,256,88]{1,2,0:T(8,128)(2,1)S(1)}, u32[]{:S(2)}, u32[]{:S(2)}) %all-to-all-start.9) | async-done | bytes 720928 | tf_op jit(solution)/shard_map/all_to_all | solution.py:41
  183.8 0.1 convert_reduce_fusion
  183.9 0.8 broadcast_in_dim.29
  184.7 3.5 %all-to-all-start.11 = ((bf16[16,128,88]{1,2,0:T(8,128)(2,1)}), bf16[16,128,88]{1,2,0:T(8,128)(2,1)S(1)}, u32[]{:S(2)}, u32[]{:S(2)}) async-start(bf16[16,128,88]{1,2,0:T(8,128)(2,1)} %broadcast_in_dim.29), calls=%async_computation.11 | async-start | bytes 720896 | tf_op jit(solution)/shard_map/all_to_all | solution.py:14
  188.2 0.3 copy.54
  188.6 7.7 %all-to-all-done.11 = bf16[16,128,88]{1,2,0:T(8,128)(2,1)S(1)} async-done(((bf16[16,128,88]{1,2,0:T(8,128)(2,1)}), bf16[16,128,88]{1,2,0:T(8,128)(2,1)S(1)}, u32[]{:S(2)}, u32[]{:S(2)}) %all-to-all-start.11) | async-done | bytes 360480 | tf_op jit(solution)/shard_map/all_to_all | solution.py:14
  196.3 1.0 convolution_bitcast_fusion
  197.3 7.3 %all-to-all-start.12 = ((f32[8,128,32]{1,2,0:T(8,128)}), f32[8,128,32]{1,2,0:T(8,128)S(1)}, u32[]{:S(2)}, u32[]{:S(2)}) async-start(f32[8,128,32]{1,2,0:T(8,128)} %convolution_bitcast_fusion), calls=%async_computation.12 | async-start | bytes 262144 | tf_op jit(solution)/shard_map/all_to_all | solution.py:35
  204.6 0.6 fusion.23
  205.2 0.6 fusion.11
  205.9 4.0 %all-to-all-done.12 = f32[8,128,32]{1,2,0:T(8,128)S(1)} async-done(((f32[8,128,32]{1,2,0:T(8,128)}), f32[8,128,32]{1,2,0:T(8,128)S(1)}, u32[]{:S(2)}, u32[]{:S(2)}) %all-to-all-start.12) | async-done | bytes 131104 | tf_op jit(solution)/shard_map/all_to_all | solution.py:35
  209.9 0.6 add_convert_fusion
  (93 shorter events, 1.6 us)
Async XLA Ops:
  0.6 12.2 %copy-start = (bf16[256,1408]{1,0:T(8,128)(2,1)S(1)}, bf16[256,1408]{1,0:T(8,128)(2,1)}, u32[]{:S(2)}) copy-start(bf16[256,1408]{1,0:T(8,128)(2,1)} %param.30) | copy-start | bytes 2162692
  2.1 10.6 %all-to-all-start = ((bf16[8,128,32]{1,2,0:T(8,128)(2,1)}), bf16[8,128,32]{1,2,0:T(8,128)(2,1)S(1)}, u32[]{:S(2)}, u32[]{:S(2)}) async-start(bf16[8,128,32]{1,2,0:T(8,128)(2,1)} %broadcast_in_dim.20), calls=%async_computation | async-start | bytes 131072 | tf_op jit(solution)/shard_map/all_to_all | solution.py:14
  12.8 37.2 %copy-start.1 = (bf16[1408,256]{1,0:T(8,128)(2,1)S(1)}, bf16[1408,256]{1,0:T(8,128)(2,1)}, u32[]{:S(2)}) copy-start(bf16[1408,256]{1,0:T(8,128)(2,1)} %param.31) | copy-start | bytes 2162692
  15.2 14.1 %all-to-all-start.2 = ((bf16[16,128,1]{1,2,0:T(2,128)(2,1)}), bf16[16,128,1]{1,2,0:T(2,128)(2,1)S(1)}, u32[]{:S(2)}, u32[]{:S(2)}) async-start(bf16[16,128,1]{1,2,0:T(2,128)(2,1)} %transpose.92), calls=%async_computation.2 | async-start | bytes 16384 | tf_op jit(solution)/shard_map/all_to_all | solution.py:41
  23.0 48.1 %copy-start.13 = (bf16[128,32]{0,1:T(8,128)(2,1)S(1)}, bf16[128,32]{0,1:T(8,128)(2,1)}, u32[]{:S(2)}) copy-start(bf16[128,32]{0,1:T(8,128)(2,1)} %param.27) | copy-start | bytes 24580
  23.0 52.9 %copy-start.21 = (bf16[256]{0:T(256)(128)(2,1)S(1)}, bf16[256]{0:T(256)(128)(2,1)}, u32[]{:S(2)}) copy-start(bf16[256]{0:T(256)(128)(2,1)} %param.32) | copy-start | bytes 1540
  29.3 52.0 %copy-start.6 = (bf16[256,1024]{1,0:T(8,128)(2,1)S(1)}, bf16[256,1024]{1,0:T(8,128)(2,1)}, u32[]{:S(2)}) copy-start(bf16[256,1024]{1,0:T(8,128)(2,1)} %param.34) | copy-start | bytes 1572868
  29.3 15.4 %all-to-all-start.1 = ((bf16[16,256,88]{1,2,0:T(8,128)(2,1)}), bf16[16,256,88]{1,2,0:T(8,128)(2,1)S(1)}, u32[]{:S(2)}, u32[]{:S(2)}) async-start(bf16[16,256,88]{1,2,0:T(8,128)(2,1)} %bitcast.3), calls=%async_computation.1 | async-start | bytes 1441792 | tf_op jit(solution)/shard_map/all_to_all | solution.py:41
  33.1 48.5 %copy-start.7 = (bf16[256,1024]{1,0:T(8,128)(2,1)S(1)}, bf16[256,1024]{1,0:T(8,128)(2,1)}, u32[]{:S(2)}) copy-start(bf16[256,1024]{1,0:T(8,128)(2,1)} %param.33) | copy-start | bytes 1572868
  44.8 37.0 %copy-start.9 = (bf16[256,256]{1,0:T(8,128)(2,1)S(1)}, bf16[256,256]{1,0:T(8,128)(2,1)}, u32[]{:S(2)}) copy-start(bf16[256,256]{1,0:T(8,128)(2,1)} %param.36) | copy-start | bytes 393220
  45.6 36.4 %copy-start.10 = (bf16[256,256]{1,0:T(8,128)(2,1)S(1)}, bf16[256,256]{1,0:T(8,128)(2,1)}, u32[]{:S(2)}) copy-start(bf16[256,256]{1,0:T(8,128)(2,1)} %param.35) | copy-start | bytes 393220
  45.6 12.5 %all-to-all-start.3 = ((bf16[16,128,88]{1,2,0:T(8,128)(2,1)}), bf16[16,128,88]{1,2,0:T(8,128)(2,1)}, u32[]{:S(2)}, u32[]{:S(2)}) async-start(bf16[16,128,88]{1,2,0:T(8,128)(2,1)} %broadcast_in_dim.21), calls=%async_computation.3 | async-start | bytes 720896 | tf_op jit(solution)/shard_map/all_to_all | solution.py:14
  50.0 32.3 %copy-start.14 = (bf16[256,16]{0,1:T(8,128)(2,1)S(1)}, bf16[256,16]{0,1:T(8,128)(2,1)}, u32[]{:S(2)}) copy-start(bf16[256,16]{0,1:T(8,128)(2,1)} %param.37) | copy-start | bytes 24580
  71.8 9.0 %all-to-all-start.5 = ((bf16[8,128,32]{1,2,0:T(8,128)(2,1)}), bf16[8,128,32]{1,2,0:T(8,128)(2,1)S(1)}, u32[]{:S(2)}, u32[]{:S(2)}) async-start(bf16[8,128,32]{1,2,0:T(8,128)(2,1)} %broadcast_in_dim.22), calls=%async_computation.5 | async-start | bytes 131072 | tf_op jit(solution)/shard_map/all_to_all | solution.py:14
  81.3 6.4 %copy-start.15 = (bf16[4,1024]{1,0:T(4,128)(2,1)S(1)}, bf16[4,1024]{1,0:T(4,128)(2,1)}, u32[]{:S(2)}) copy-start(bf16[4,1024]{1,0:T(4,128)(2,1)} %param.41) | copy-start | bytes 24580
  81.3 6.4 %copy-start.22 = (f32[16]{0:T(128)S(1)}, f32[16]{0:T(128)}, u32[]{:S(2)}) copy-start(f32[16]{0:T(128)} %param.39) | copy-start | bytes 196
  81.3 6.4 %copy-start.16 = (bf16[4,256]{1,0:T(4,128)(2,1)S(1)}, bf16[4,256]{1,0:T(4,128)(2,1)}, u32[]{:S(2)}) copy-start(bf16[4,256]{1,0:T(4,128)(2,1)} %param.42) | copy-start | bytes 6148
  81.3 6.4 %copy-start.17 = (bf16[4,256]{1,0:T(4,128)(2,1)S(1)}, bf16[4,256]{1,0:T(4,128)(2,1)}, u32[]{:S(2)}) copy-start(bf16[4,256]{1,0:T(4,128)(2,1)} %param.43) | copy-start | bytes 6148
  81.3 6.4 %copy-start.20 = (f32[16]{0:T(128)S(1)}, f32[16]{0:T(128)}, u32[]{:S(2)}) copy-start(f32[16]{0:T(128)} %param.40) | copy-start | bytes 196
  81.4 6.6 %copy-start.18 = (bf16[1024]{0:T(1024)(128)(2,1)S(1)}, bf16[1024]{0:T(1024)(128)(2,1)}, u32[]{:S(2)}) copy-start(bf16[1024]{0:T(1024)(128)(2,1)} %param.48) | copy-start | bytes 6148
  81.9 27.0 %copy-start.8 = (bf16[8,3,1024]{2,0,1:T(8,128)(2,1)S(1)}, bf16[8,3,1024]{2,0,1:T(8,128)(2,1)}, u32[]{:S(2)}) copy-start(bf16[8,3,1024]{2,0,1:T(8,128)(2,1)} %param.44) | copy-start | bytes 147460
  81.9 27.1 %copy-start.11 = (bf16[8,3,256]{2,0,1:T(8,128)(2,1)S(1)}, bf16[8,3,256]{2,0,1:T(8,128)(2,1)}, u32[]{:S(2)}) copy-start(bf16[8,3,256]{2,0,1:T(8,128)(2,1)} %param.46) | copy-start | bytes 36868
  81.9 27.1 %copy-start.12 = (bf16[8,3,256]{2,0,1:T(8,128)(2,1)S(1)}, bf16[8,3,256]{2,0,1:T(8,128)(2,1)}, u32[]{:S(2)}) copy-start(bf16[8,3,256]{2,0,1:T(8,128)(2,1)} %param.45) | copy-start | bytes 36868
  82.1 27.0 %copy-start.19 = (f32[16]{0:T(128)S(1)}, f32[16]{0:T(128)}, u32[]{:S(2)}) copy-start(f32[16]{0:T(128)} %param.38) | copy-start | bytes 196
  83.9 24.5 %all-to-all-start.6 = ((f32[16,8,2577]{2,1,0:T(8,128)}), f32[16,8,2577]{2,1,0:T(8,128)S(1)}, u32[]{:S(2)}, u32[]{:S(2)}) async-start(f32[16,8,2577]{2,1,0:T(8,128)} %concatenate.23), calls=%async_computation.6 | async-start | bytes 2752512 | tf_op jit(solution)/shard_map/all_to_all | solution.py:35
  109.3 21.7 %copy-start.5 = (bf16[1024,256]{1,0:T(8,128)(2,1)S(1)}, bf16[1024,256]{1,0:T(8,128)(2,1)}, u32[]{:S(2)}) copy-start(bf16[1024,256]{1,0:T(8,128)(2,1)} %param.49) | copy-start | bytes 1572868
  109.3 41.9 %copy-start.23 = (bf16[256]{0:T(256)(128)(2,1)S(1)}, bf16[256]{0:T(256)(128)(2,1)}, u32[]{:S(2)}) copy-start(bf16[256]{0:T(256)(128)(2,1)} %param.50) | copy-start | bytes 1540
  109.3 46.8 %copy-start.2 = (bf16[256,1408]{1,0:T(8,128)(2,1)S(1)}, bf16[256,1408]{1,0:T(8,128)(2,1)}, u32[]{:S(2)}) copy-start(bf16[256,1408]{1,0:T(8,128)(2,1)} %param.52) | copy-start | bytes 2162692
  109.3 47.2 %copy-start.3 = (bf16[256,1408]{1,0:T(8,128)(2,1)S(1)}, bf16[256,1408]{1,0:T(8,128)(2,1)}, u32[]{:S(2)}) copy-start(bf16[256,1408]{1,0:T(8,128)(2,1)} %param.51) | copy-start | bytes 2162692
  147.1 9.0 %all-to-all-start.8 = ((bf16[8,128,32]{1,2,0:T(8,128)(2,1)}), bf16[8,128,32]{1,2,0:T(8,128)(2,1)S(1)}, u32[]{:S(2)}, u32[]{:S(2)}) async-start(bf16[8,128,32]{1,2,0:T(8,128)(2,1)} %broadcast_in_dim.28), calls=%async_computation.8 | async-start | bytes 131072 | tf_op jit(solution)/shard_map/all_to_all | solution.py:14
  156.2 32.1 %copy-start.4 = (bf16[1408,256]{1,0:T(8,128)(2,1)S(1)}, bf16[1408,256]{1,0:T(8,128)(2,1)}, u32[]{:S(2)}) copy-start(bf16[1408,256]{1,0:T(8,128)(2,1)} %param.53) | copy-start | bytes 2162692
  157.4 11.1 %all-to-all-start.10 = ((bf16[16,128,1]{1,2,0:T(2,128)(2,1)}), bf16[16,128,1]{1,2,0:T(2,128)(2,1)S(1)}, u32[]{:S(2)}, u32[]{:S(2)}) async-start(bf16[16,128,1]{1,2,0:T(2,128)(2,1)} %transpose.97), calls=%async_computation.10 | async-start | bytes 16384 | tf_op jit(solution)/shard_map/all_to_all | solution.py:41
  168.5 15.3 %all-to-all-start.9 = ((bf16[16,256,88]{1,2,0:T(8,128)(2,1)}), bf16[16,256,88]{1,2,0:T(8,128)(2,1)S(1)}, u32[]{:S(2)}, u32[]{:S(2)}) async-start(bf16[16,256,88]{1,2,0:T(8,128)(2,1)} %bitcast.28), calls=%async_computation.9 | async-start | bytes 1441792 | tf_op jit(solution)/shard_map/all_to_all | solution.py:41
  184.7 11.6 %all-to-all-start.11 = ((bf16[16,128,88]{1,2,0:T(8,128)(2,1)}), bf16[16,128,88]{1,2,0:T(8,128)(2,1)S(1)}, u32[]{:S(2)}, u32[]{:S(2)}) async-start(bf16[16,128,88]{1,2,0:T(8,128)(2,1)} %broadcast_in_dim.29), calls=%async_computation.11 | async-start | bytes 720896 | tf_op jit(solution)/shard_map/all_to_all | solution.py:14
  197.3 12.6 %all-to-all-start.12 = ((f32[8,128,32]{1,2,0:T(8,128)}), f32[8,128,32]{1,2,0:T(8,128)S(1)}, u32[]{:S(2)}, u32[]{:S(2)}) async-start(f32[8,128,32]{1,2,0:T(8,128)} %convolution_bitcast_fusion), calls=%async_computation.12 | async-start | bytes 262144 | tf_op jit(solution)/shard_map/all_to_all | solution.py:35
where the time goes:
time: 212 us; the launch traced here: 211 us
  waiting for transfers between devices  87.4 us (41%)
  starting transfers between devices  52.7 us (25%)
  blocking collectives  42.8 us (20%)
  local copies, waits for them, and re-layouts  10.9 us (5%)
  other arithmetic  9.52 us (4%)
  matrix products  5.91 us (3%)
    all_to_all x4, waiting for transfers between devices, sum_at_owner(): lax.all_to_all(blocks, axis, split_axis=0, concat_axis=0, tiled=True)  33.5 us
    all_to_all x5, waiting for transfers between devices, copy_for_each(): return lax.all_to_all(copies, axis, split_axis=0, concat_axis=0, tiled=True)  29.4 us
    all_to_all x2, blocking collectives, sent_and_summed(): lax.all_to_all(in_blocks(shard, dim, length), axis, 0, 0, tiled=True)  26.8 us
    all_to_all x2, waiting for transfers between devices, sent_and_summed(): lax.all_to_all(in_blocks(shard, dim, length), axis, 0, 0, tiled=True)  24.6 us
    all_to_all x5, starting transfers between devices, copy_for_each(): return lax.all_to_all(copies, axis, split_axis=0, concat_axis=0, tiled=True)  21.9 us
    all_to_all x4, starting transfers between devices, sum_at_owner(): lax.all_to_all(blocks, axis, split_axis=0, concat_axis=0, tiled=True)  19.8 us
    all_gather x1, blocking collectives, local(): lax.all_gather(mixer_rows, 'kv', axis=0, tiled=True)  16 us
    all_to_all x2, starting transfers between devices, sent_and_summed(): lax.all_to_all(in_blocks(shard, dim, length), axis, 0, 0, tiled=True)  11 us
  transfers between devices with their start and end apart: 11, of which 11 were waited for; matrix products, arithmetic and copies ran while one was open for 2% of the time, Pallas kernels for 0%

commit v1 on v0

--- a/solution.py
+++ b/solution.py
@@ -7,6 +7,14 @@
 HEAD_DIM = 64
 STATE = 128
 EPS = 1e-06
+
+
+def gather_from_all(value, axis, dim):
+    count = lax.axis_size(axis)
+    repeats = [count if d == dim else 1 for d in range(value.ndim)]
+    return lax.all_to_all(
+        jnp.tile(value, repeats), axis, split_axis=dim, concat_axis=dim, tiled=True
+    )
 
 
 def copy_for_each(shard, axis):
@@ -201,9 +209,7 @@
     )
     mixer_rows = (normed * group_gain.astype(jnp.float32)[None, :]).astype(jnp.bfloat16)
     back_part = jnp.dot(
-        lax.all_gather(mixer_rows, "kv", axis=0, tiled=True),
-        mixer_out,
-        preferred_element_type=jnp.float32,
+        gather_from_all(mixer_rows, "kv", 0), mixer_out, preferred_element_type=jnp.float32
     )
     returned = column_sums(back_part)
     middle = (first_out.astype(jnp.float32) + returned).astype(jnp.bfloat16)

time: 212 us -> 202 us (0.953)
  blocking collectives: 42.8 us -> 21.7 us
  waiting for transfers between devices: 87.4 us -> 94.3 us
  starting transfers between devices: 52.7 us -> 55.7 us
    all_gather x1 -> x0, blocking collectives: 16 us -> none  [local(): lax.all_gather(mixer_rows, 'kv', axis=0, tiled=True)]
    all_to_all x0 -> x1, waiting for transfers between devices: none -> 7.43 us  [gather_from_all(): lax.all_to_all(jnp.tile(value, repeats), axis, split_axis=dim, concat_axi...]
    all_to_all x2, blocking collectives: 26.8 us -> 21.7 us  [sent_and_summed(): lax.all_to_all(in_blocks(shard, dim, length), axis, 0, 0, tiled=True)]
    all_to_all x0 -> x1, starting transfers between devices: none -> 4.36 us  [gather_from_all(): lax.all_to_all(jnp.tile(value, repeats), axis, split_axis=dim, concat_axi...]
  transfers between devices with their start and end apart: 11 -> 12, of which waited for: 11 -> 12; matrix products, arithmetic and copies ran while one was open for 2% -> 3% of each run, Pallas kernels for 0% -> 0%
where the time goes in v1:
time: 202 us; the launch traced here: 201 us
  waiting for transfers between devices  94.3 us (47%)
  starting transfers between devices  55.7 us (28%)
  blocking collectives  21.7 us (11%)
  local copies, waits for them, and re-layouts  11.8 us (6%)
  other arithmetic  10.1 us (5%)
  matrix products  5.87 us (3%)
    all_to_all x4, waiting for transfers between devices, sum_at_owner(): lax.all_to_all(blocks, axis, split_axis=0, concat_axis=0, tiled=True)  33.6 us
    all_to_all x5, waiting for transfers between devices, copy_for_each(): return lax.all_to_all(copies, axis, split_axis=0, concat_axis=0, tiled=True)  28.7 us
    all_to_all x2, waiting for transfers between devices, sent_and_summed(): lax.all_to_all(in_blocks(shard, dim, length), axis, 0, 0, tiled=True)  24.5 us
    all_to_all x5, starting transfers between devices, copy_for_each(): return lax.all_to_all(copies, axis, split_axis=0, concat_axis=0, tiled=True)  21.9 us
    all_to_all x2, blocking collectives, sent_and_summed(): lax.all_to_all(in_blocks(shard, dim, length), axis, 0, 0, tiled=True)  21.7 us
    all_to_all x4, starting transfers between devices, sum_at_owner(): lax.all_to_all(blocks, axis, split_axis=0, concat_axis=0, tiled=True)  18.6 us
    all_to_all x2, starting transfers between devices, sent_and_summed(): lax.all_to_all(in_blocks(shard, dim, length), axis, 0, 0, tiled=True)  10.9 us
    all_to_all x1, waiting for transfers between devices, gather_from_all(): lax.all_to_all(jnp.tile(value, repeats), axis, split_axis=dim, concat_axi...  7.43 us
  transfers between devices with their start and end apart: 12, of which 12 were waited for; matrix products, arithmetic and copies ran while one was open for 3% of the time, Pallas kernels for 0%

profile of v1, /device:TPU:1, one launch (start us, length us, event | category | flops | bytes accessed | tf_op | source)
XLA Modules:
  0.0 200.8 jit_solution(9271830879235140457)
XLA Ops:
  0.6 1.4 broadcast_in_dim.20
  2.1 5.8 %all-to-all-start = ((bf16[8,128,32]{1,2,0:T(8,128)(2,1)}), bf16[8,128,32]{1,2,0:T(8,128)(2,1)S(1)}, u32[]{:S(2)}, u32[]{:S(2)}) async-start(bf16[8,128,32]{1,2,0:T(8,128)(2,1)} %broadcast_in_dim.20), calls=%async_computation | async-start | bytes 131072 | tf_op jit(solution)/shard_map/all_to_all | solution.py:22
  7.8 0.7 convert_element_type.166
  8.5 4.2 %all-to-all-done = bf16[8,128,32]{1,2,0:T(8,128)(2,1)S(1)} async-done(((bf16[8,128,32]{1,2,0:T(8,128)(2,1)}), bf16[8,128,32]{1,2,0:T(8,128)(2,1)S(1)}, u32[]{:S(2)}, u32[]{:S(2)}) %all-to-all-start) | async-done | bytes 65568 | tf_op jit(solution)/shard_map/all_to_all | solution.py:22
  12.8 0.3 convolution_convert_fusion.2
  13.1 1.4 convolution_convert_fusion.3
  14.6 0.6 transpose.94
  15.2 7.8 %all-to-all-start.2 = ((bf16[16,128,1]{1,2,0:T(2,128)(2,1)}), bf16[16,128,1]{1,2,0:T(2,128)(2,1)S(1)}, u32[]{:S(2)}, u32[]{:S(2)}) async-start(bf16[16,128,1]{1,2,0:T(2,128)(2,1)} %transpose.94), calls=%async_computation.2 | async-start | bytes 16384 | tf_op jit(solution)/shard_map/all_to_all | solution.py:49
  23.1 1.1 copy.48
  24.2 5.1 %all-to-all-done.2 = bf16[16,128,1]{1,2,0:T(2,128)(2,1)S(1)} async-done(((bf16[16,128,1]{1,2,0:T(2,128)(2,1)}), bf16[16,128,1]{1,2,0:T(2,128)(2,1)S(1)}, u32[]{:S(2)}, u32[]{:S(2)}) %all-to-all-start.2) | async-done | bytes 4128 | tf_op jit(solution)/shard_map/all_to_all | solution.py:49
  29.3 3.7 %all-to-all-start.1 = ((bf16[16,256,88]{1,2,0:T(8,128)(2,1)}), bf16[16,256,88]{1,2,0:T(8,128)(2,1)S(1)}, u32[]{:S(2)}, u32[]{:S(2)}) async-start(bf16[16,256,88]{1,2,0:T(8,128)(2,1)} %bitcast.3), calls=%async_computation.1 | async-start | bytes 1441792 | tf_op jit(solution)/shard_map/all_to_all | solution.py:49
  33.1 11.6 %all-to-all-done.1 = bf16[16,256,88]{1,2,0:T(8,128)(2,1)S(1)} async-done(((bf16[16,256,88]{1,2,0:T(8,128)(2,1)}), bf16[16,256,88]{1,2,0:T(8,128)(2,1)S(1)}, u32[]{:S(2)}, u32[]{:S(2)}) %all-to-all-start.1) | async-done | bytes 720928 | tf_op jit(solution)/shard_map/all_to_all | solution.py:49
  44.7 0.1 convert_reduce_fusion.1
  44.9 0.8 broadcast_in_dim.21
  45.7 4.3 %all-to-all-start.3 = ((bf16[16,128,88]{1,2,0:T(8,128)(2,1)}), bf16[16,128,88]{1,2,0:T(8,128)(2,1)}, u32[]{:S(2)}, u32[]{:S(2)}) async-start(bf16[16,128,88]{1,2,0:T(8,128)(2,1)} %broadcast_in_dim.21), calls=%async_computation.3 | async-start | bytes 720896 | tf_op jit(solution)/shard_map/all_to_all | solution.py:22
  50.0 0.3 copy.49
  50.4 7.8 %all-to-all-done.3 = bf16[16,128,88]{1,2,0:T(8,128)(2,1)} async-done(((bf16[16,128,88]{1,2,0:T(8,128)(2,1)}), bf16[16,128,88]{1,2,0:T(8,128)(2,1)}, u32[]{:S(2)}, u32[]{:S(2)}) %all-to-all-start.3) | async-done | bytes 360480 | tf_op jit(solution)/shard_map/all_to_all | solution.py:22
  58.1 1.3 convolution_bitcast_fusion.2
  59.5 11.7 %all_to_all.74 = f32[8,128,32]{1,2,0:T(8,128)S(1)} all-to-all(f32[8,128,32]{1,2,0:T(8,128)S(1)} %convolution_bitcast_fusion.2), channel_id=1, replica_groups=mesh['kv'=16,'tp'=8] {'tp'}, dimensions={0} | all-to-all | bytes 262144 | tf_op jit(solution)/shard_map/all_to_all | solution.py:43
  71.2 0.6 broadcast_in_dim.22
  71.8 4.1 %all-to-all-start.5 = ((bf16[8,128,32]{1,2,0:T(8,128)(2,1)}), bf16[8,128,32]{1,2,0:T(8,128)(2,1)S(1)}, u32[]{:S(2)}, u32[]{:S(2)}) async-start(bf16[8,128,32]{1,2,0:T(8,128)(2,1)} %broadcast_in_dim.22), calls=%async_computation.5 | async-start | bytes 131072 | tf_op jit(solution)/shard_map/all_to_all | solution.py:22
  76.0 4.9 %all-to-all-done.5 = bf16[8,128,32]{1,2,0:T(8,128)(2,1)S(1)} async-done(((bf16[8,128,32]{1,2,0:T(8,128)(2,1)}), bf16[8,128,32]{1,2,0:T(8,128)(2,1)S(1)}, u32[]{:S(2)}, u32[]{:S(2)}) %all-to-all-start.5) | async-done | bytes 65568 | tf_op jit(solution)/shard_map/all_to_all | solution.py:22
  80.8 0.2 copy.51
  81.1 0.2 reshape.181
  81.3 0.2 fusion
  81.6 0.2 fusion.2
  81.9 0.2 fusion.10
  82.1 0.2 fusion.8
  82.3 0.1 fusion.28
  82.5 0.2 concatenate.28
  82.7 1.3 concatenate.23
  84.0 3.7 %all-to-all-start.6 = ((f32[16,8,2577]{2,1,0:T(8,128)}), f32[16,8,2577]{2,1,0:T(8,128)S(1)}, u32[]{:S(2)}, u32[]{:S(2)}) async-start(f32[16,8,2577]{2,1,0:T(8,128)} %concatenate.23), calls=%async_computation.6 | async-start | bytes 2752512 | tf_op jit(solution)/shard_map/all_to_all | solution.py:43
  87.9 20.5 %all-to-all-done.6 = f32[16,8,2577]{2,1,0:T(8,128)S(1)} async-done(((f32[16,8,2577]{2,1,0:T(8,128)}), f32[16,8,2577]{2,1,0:T(8,128)S(1)}, u32[]{:S(2)}, u32[]{:S(2)}) %all-to-all-start.6) | async-done | bytes 1319456 | tf_op jit(solution)/shard_map/all_to_all | solution.py:43
  108.5 0.2 fusion.34
  109.3 5.2 %multiply_reduce_fusion = (f32[8,16,64]{2,1,0:T(8,128)S(1)}, f32[8,16,64,128]{3,2,1,0:T(8,128)}) fusion(f32[8,16,128]{2,1,0:T(8,128)S(1)} %broadcast_bitcast_fusion, f32[8,16,128]{2,1,0:T(8,128)S(1)} %broadcast_bitcast_fusion.1, f32[8,16,64]{2,1,0:T(8,128)S(1)} %multiply_multiply_fusion, f32[8,16,64,128]{3,2,1,0:T(8,128)} %param.47, ...), kind=kLoop, calls=%fused_computation | loop fusion | flops 5234688 | bytes 8585728 | tf_op jit(solution)/shard_map/reduce_sum | solution.py:141
  114.9 0.7 tile.2
  115.6 4.4 %all-to-all-start.7 = ((bf16[16,8,1024]{2,1,0:T(8,128)(2,1)}), bf16[16,8,1024]{2,1,0:T(8,128)(2,1)S(1)}, u32[]{:S(2)}, u32[]{:S(2)}) async-start(bf16[16,8,1024]{2,1,0:T(8,128)(2,1)} %tile.2), calls=%async_computation.7 | async-start | bytes 524288 | tf_op jit(solution)/shard_map/all_to_all | solution.py:15
  120.0 0.2 copy.53
  120.2 7.4 %all-to-all-done.7 = bf16[16,8,1024]{2,1,0:T(8,128)(2,1)S(1)} async-done(((bf16[16,8,1024]{2,1,0:T(8,128)(2,1)}), bf16[16,8,1024]{2,1,0:T(8,128)(2,1)S(1)}, u32[]{:S(2)}, u32[]{:S(2)}) %all-to-all-start.7) | async-done | bytes 262176 | tf_op jit(solution)/shard_map/all_to_all | solution.py:15
  127.6 0.3 convolution_bitcast_fusion.1
  127.9 10.0 %all_to_all.75 = f32[8,128,32]{1,2,0:T(8,128)S(1)} all-to-all(f32[8,128,32]{1,2,0:T(8,128)S(1)} %convolution_bitcast_fusion.1), channel_id=1, replica_groups=mesh['kv'=16,'tp'=8] {'tp'}, dimensions={0} | all-to-all | bytes 262144 | tf_op jit(solution)/shard_map/all_to_all | solution.py:43
  138.0 0.6 broadcast_in_dim.28
  138.6 4.1 %all-to-all-start.9 = ((bf16[8,128,32]{1,2,0:T(8,128)(2,1)}), bf16[8,128,32]{1,2,0:T(8,128)(2,1)S(1)}, u32[]{:S(2)}, u32[]{:S(2)}) async-start(bf16[8,128,32]{1,2,0:T(8,128)(2,1)} %broadcast_in_dim.28), calls=%async_computation.9 | async-start | bytes 131072 | tf_op jit(solution)/shard_map/all_to_all | solution.py:22
  142.7 0.7 convert_element_type.201
  143.4 4.2 %all-to-all-done.9 = bf16[8,128,32]{1,2,0:T(8,128)(2,1)S(1)} async-done(((bf16[8,128,32]{1,2,0:T(8,128)(2,1)}), bf16[8,128,32]{1,2,0:T(8,128)(2,1)S(1)}, u32[]{:S(2)}, u32[]{:S(2)}) %all-to-all-start.9) | async-done | bytes 65568 | tf_op jit(solution)/shard_map/all_to_all | solution.py:22
  147.7 0.3 convolution_convert_fusion
  148.1 0.3 convolution_convert_fusion.1
  148.4 0.6 transpose.99
  149.0 3.5 %all-to-all-start.11 = ((bf16[16,128,1]{1,2,0:T(2,128)(2,1)}), bf16[16,128,1]{1,2,0:T(2,128)(2,1)S(1)}, u32[]{:S(2)}, u32[]{:S(2)}) async-start(bf16[16,128,1]{1,2,0:T(2,128)(2,1)} %transpose.99), calls=%async_computation.11 | async-start | bytes 16384 | tf_op jit(solution)/shard_map/all_to_all | solution.py:49
  152.6 1.1 copy.54
  153.7 5.1 %all-to-all-done.11 = bf16[16,128,1]{1,2,0:T(2,128)(2,1)S(1)} async-done(((bf16[16,128,1]{1,2,0:T(2,128)(2,1)}), bf16[16,128,1]{1,2,0:T(2,128)(2,1)S(1)}, u32[]{:S(2)}, u32[]{:S(2)}) %all-to-all-start.11) | async-done | bytes 4128 | tf_op jit(solution)/shard_map/all_to_all | solution.py:49
  158.8 3.6 %all-to-all-start.10 = ((bf16[16,256,88]{1,2,0:T(8,128)(2,1)}), bf16[16,256,88]{1,2,0:T(8,128)(2,1)S(1)}, u32[]{:S(2)}, u32[]{:S(2)}) async-start(bf16[16,256,88]{1,2,0:T(8,128)(2,1)} %bitcast.31), calls=%async_computation.10 | async-start | bytes 1441792 | tf_op jit(solution)/shard_map/all_to_all | solution.py:49
  162.5 11.8 %all-to-all-done.10 = bf16[16,256,88]{1,2,0:T(8,128)(2,1)S(1)} async-done(((bf16[16,256,88]{1,2,0:T(8,128)(2,1)}), bf16[16,256,88]{1,2,0:T(8,128)(2,1)S(1)}, u32[]{:S(2)}, u32[]{:S(2)}) %all-to-all-start.10) | async-done | bytes 720928 | tf_op jit(solution)/shard_map/all_to_all | solution.py:49
  174.2 0.1 convert_reduce_fusion
  174.4 0.8 broadcast_in_dim.29
  175.2 3.5 %all-to-all-start.12 = ((bf16[16,128,88]{1,2,0:T(8,128)(2,1)}), bf16[16,128,88]{1,2,0:T(8,128)(2,1)S(1)}, u32[]{:S(2)}, u32[]{:S(2)}) async-start(bf16[16,128,88]{1,2,0:T(8,128)(2,1)} %broadcast_in_dim.29), calls=%async_computation.12 | async-start | bytes 720896 | tf_op jit(solution)/shard_map/all_to_all | solution.py:22
  178.7 0.3 copy.55
  179.1 7.7 %all-to-all-done.12 = bf16[16,128,88]{1,2,0:T(8,128)(2,1)S(1)} async-done(((bf16[16,128,88]{1,2,0:T(8,128)(2,1)}), bf16[16,128,88]{1,2,0:T(8,128)(2,1)S(1)}, u32[]{:S(2)}, u32[]{:S(2)}) %all-to-all-start.12) | async-done | bytes 360480 | tf_op jit(solution)/shard_map/all_to_all | solution.py:22
  186.7 1.0 convolution_bitcast_fusion
  187.8 7.2 %all-to-all-start.13 = ((f32[8,128,32]{1,2,0:T(8,128)}), f32[8,128,32]{1,2,0:T(8,128)S(1)}, u32[]{:S(2)}, u32[]{:S(2)}) async-start(f32[8,128,32]{1,2,0:T(8,128)} %convolution_bitcast_fusion), calls=%async_computation.13 | async-start | bytes 262144 | tf_op jit(solution)/shard_map/all_to_all | solution.py:43
  194.9 0.6 fusion.24
  195.5 0.6 fusion.12
  196.2 4.0 %all-to-all-done.13 = f32[8,128,32]{1,2,0:T(8,128)S(1)} async-done(((f32[8,128,32]{1,2,0:T(8,128)}), f32[8,128,32]{1,2,0:T(8,128)S(1)}, u32[]{:S(2)}, u32[]{:S(2)}) %all-to-all-start.13) | async-done | bytes 131104 | tf_op jit(solution)/shard_map/all_to_all | solution.py:43
  200.2 0.6 add_convert_fusion
  (98 shorter events, 1.9 us)
Async XLA Ops:
  0.6 12.2 %copy-start = (bf16[256,1408]{1,0:T(8,128)(2,1)S(1)}, bf16[256,1408]{1,0:T(8,128)(2,1)}, u32[]{:S(2)}) copy-start(bf16[256,1408]{1,0:T(8,128)(2,1)} %param.30) | copy-start | bytes 2162692
  2.1 10.6 %all-to-all-start = ((bf16[8,128,32]{1,2,0:T(8,128)(2,1)}), bf16[8,128,32]{1,2,0:T(8,128)(2,1)S(1)}, u32[]{:S(2)}, u32[]{:S(2)}) async-start(bf16[8,128,32]{1,2,0:T(8,128)(2,1)} %broadcast_in_dim.20), calls=%async_computation | async-start | bytes 131072 | tf_op jit(solution)/shard_map/all_to_all | solution.py:22
  12.8 37.2 %copy-start.1 = (bf16[1408,256]{1,0:T(8,128)(2,1)S(1)}, bf16[1408,256]{1,0:T(8,128)(2,1)}, u32[]{:S(2)}) copy-start(bf16[1408,256]{1,0:T(8,128)(2,1)} %param.31) | copy-start | bytes 2162692
  15.2 14.1 %all-to-all-start.2 = ((bf16[16,128,1]{1,2,0:T(2,128)(2,1)}), bf16[16,128,1]{1,2,0:T(2,128)(2,1)S(1)}, u32[]{:S(2)}, u32[]{:S(2)}) async-start(bf16[16,128,1]{1,2,0:T(2,128)(2,1)} %transpose.94), calls=%async_computation.2 | async-start | bytes 16384 | tf_op jit(solution)/shard_map/all_to_all | solution.py:49
  23.0 48.1 %copy-start.15 = (bf16[128,32]{0,1:T(8,128)(2,1)S(1)}, bf16[128,32]{0,1:T(8,128)(2,1)}, u32[]{:S(2)}) copy-start(bf16[128,32]{0,1:T(8,128)(2,1)} %param.27) | copy-start | bytes 24580
  23.1 52.9 %copy-start.23 = (bf16[256]{0:T(256)(128)(2,1)S(1)}, bf16[256]{0:T(256)(128)(2,1)}, u32[]{:S(2)}) copy-start(bf16[256]{0:T(256)(128)(2,1)} %param.32) | copy-start | bytes 1540
  29.3 52.0 %copy-start.5 = (bf16[256,1024]{1,0:T(8,128)(2,1)S(1)}, bf16[256,1024]{1,0:T(8,128)(2,1)}, u32[]{:S(2)}) copy-start(bf16[256,1024]{1,0:T(8,128)(2,1)} %param.34) | copy-start | bytes 1572868
  29.3 15.4 %all-to-all-start.1 = ((bf16[16,256,88]{1,2,0:T(8,128)(2,1)}), bf16[16,256,88]{1,2,0:T(8,128)(2,1)S(1)}, u32[]{:S(2)}, u32[]{:S(2)}) async-start(bf16[16,256,88]{1,2,0:T(8,128)(2,1)} %bitcast.3), calls=%async_computation.1 | async-start | bytes 1441792 | tf_op jit(solution)/shard_map/all_to_all | solution.py:49
  33.1 48.5 %copy-start.6 = (bf16[256,1024]{1,0:T(8,128)(2,1)S(1)}, bf16[256,1024]{1,0:T(8,128)(2,1)}, u32[]{:S(2)}) copy-start(bf16[256,1024]{1,0:T(8,128)(2,1)} %param.33) | copy-start | bytes 1572868
  44.9 37.0 %copy-start.9 = (bf16[256,256]{1,0:T(8,128)(2,1)S(1)}, bf16[256,256]{1,0:T(8,128)(2,1)}, u32[]{:S(2)}) copy-start(bf16[256,256]{1,0:T(8,128)(2,1)} %param.35) | copy-start | bytes 393220
  45.7 36.4 %copy-start.10 = (bf16[256,256]{1,0:T(8,128)(2,1)S(1)}, bf16[256,256]{1,0:T(8,128)(2,1)}, u32[]{:S(2)}) copy-start(bf16[256,256]{1,0:T(8,128)(2,1)} %param.36) | copy-start | bytes 393220
  45.7 12.5 %all-to-all-start.3 = ((bf16[16,128,88]{1,2,0:T(8,128)(2,1)}), bf16[16,128,88]{1,2,0:T(8,128)(2,1)}, u32[]{:S(2)}, u32[]{:S(2)}) async-start(bf16[16,128,88]{1,2,0:T(8,128)(2,1)} %broadcast_in_dim.21), calls=%async_computation.3 | async-start | bytes 720896 | tf_op jit(solution)/shard_map/all_to_all | solution.py:22
  50.0 32.3 %copy-start.16 = (bf16[256,16]{0,1:T(8,128)(2,1)S(1)}, bf16[256,16]{0,1:T(8,128)(2,1)}, u32[]{:S(2)}) copy-start(bf16[256,16]{0,1:T(8,128)(2,1)} %param.37) | copy-start | bytes 24580
  71.8 9.0 %all-to-all-start.5 = ((bf16[8,128,32]{1,2,0:T(8,128)(2,1)}), bf16[8,128,32]{1,2,0:T(8,128)(2,1)S(1)}, u32[]{:S(2)}, u32[]{:S(2)}) async-start(bf16[8,128,32]{1,2,0:T(8,128)(2,1)} %broadcast_in_dim.22), calls=%async_computation.5 | async-start | bytes 131072 | tf_op jit(solution)/shard_map/all_to_all | solution.py:22
  81.3 6.4 %copy-start.17 = (bf16[4,1024]{1,0:T(4,128)(2,1)S(1)}, bf16[4,1024]{1,0:T(4,128)(2,1)}, u32[]{:S(2)}) copy-start(bf16[4,1024]{1,0:T(4,128)(2,1)} %param.41) | copy-start | bytes 24580
  81.3 6.4 %copy-start.18 = (bf16[4,256]{1,0:T(4,128)(2,1)S(1)}, bf16[4,256]{1,0:T(4,128)(2,1)}, u32[]{:S(2)}) copy-start(bf16[4,256]{1,0:T(4,128)(2,1)} %param.42) | copy-start | bytes 6148
  81.3 6.4 %copy-start.19 = (bf16[4,256]{1,0:T(4,128)(2,1)S(1)}, bf16[4,256]{1,0:T(4,128)(2,1)}, u32[]{:S(2)}) copy-start(bf16[4,256]{1,0:T(4,128)(2,1)} %param.43) | copy-start | bytes 6148
  81.6 6.1 %copy-start.24 = (f32[16]{0:T(128)S(1)}, f32[16]{0:T(128)}, u32[]{:S(2)}) copy-start(f32[16]{0:T(128)} %param.39) | copy-start | bytes 196
  81.6 6.2 %copy-start.22 = (f32[16]{0:T(128)S(1)}, f32[16]{0:T(128)}, u32[]{:S(2)}) copy-start(f32[16]{0:T(128)} %param.40) | copy-start | bytes 196
  81.6 6.3 %copy-start.20 = (bf16[1024]{0:T(1024)(128)(2,1)S(1)}, bf16[1024]{0:T(1024)(128)(2,1)}, u32[]{:S(2)}) copy-start(bf16[1024]{0:T(1024)(128)(2,1)} %param.48) | copy-start | bytes 6148
  81.9 27.0 %copy-start.8 = (bf16[8,3,1024]{2,0,1:T(8,128)(2,1)S(1)}, bf16[8,3,1024]{2,0,1:T(8,128)(2,1)}, u32[]{:S(2)}) copy-start(bf16[8,3,1024]{2,0,1:T(8,128)(2,1)} %param.44) | copy-start | bytes 147460
  81.9 27.1 %copy-start.11 = (bf16[8,3,256]{2,0,1:T(8,128)(2,1)S(1)}, bf16[8,3,256]{2,0,1:T(8,128)(2,1)}, u32[]{:S(2)}) copy-start(bf16[8,3,256]{2,0,1:T(8,128)(2,1)} %param.46) | copy-start | bytes 36868
  81.9 27.1 %copy-start.13 = (bf16[8,3,256]{2,0,1:T(8,128)(2,1)S(1)}, bf16[8,3,256]{2,0,1:T(8,128)(2,1)}, u32[]{:S(2)}) copy-start(bf16[8,3,256]{2,0,1:T(8,128)(2,1)} %param.45) | copy-start | bytes 36868
  82.1 27.0 %copy-start.21 = (f32[16]{0:T(128)S(1)}, f32[16]{0:T(128)}, u32[]{:S(2)}) copy-start(f32[16]{0:T(128)} %param.38) | copy-start | bytes 196
  84.0 24.5 %all-to-all-start.6 = ((f32[16,8,2577]{2,1,0:T(8,128)}), f32[16,8,2577]{2,1,0:T(8,128)S(1)}, u32[]{:S(2)}, u32[]{:S(2)}) async-start(f32[16,8,2577]{2,1,0:T(8,128)} %concatenate.23), calls=%async_computation.6 | async-start | bytes 2752512 | tf_op jit(solution)/shard_map/all_to_all | solution.py:43
  109.3 10.7 %copy-start.7 = (bf16[1024,256]{1,0:T(8,128)(2,1)S(1)}, bf16[1024,256]{1,0:T(8,128)(2,1)}, u32[]{:S(2)}) copy-start(bf16[1024,256]{1,0:T(8,128)(2,1)} %param.49) | copy-start | bytes 1572868
  109.3 38.4 %copy-start.2 = (bf16[256,1408]{1,0:T(8,128)(2,1)S(1)}, bf16[256,1408]{1,0:T(8,128)(2,1)}, u32[]{:S(2)}) copy-start(bf16[256,1408]{1,0:T(8,128)(2,1)} %param.52) | copy-start | bytes 2162692
  114.5 33.5 %copy-start.3 = (bf16[256,1408]{1,0:T(8,128)(2,1)S(1)}, bf16[256,1408]{1,0:T(8,128)(2,1)}, u32[]{:S(2)}) copy-start(bf16[256,1408]{1,0:T(8,128)(2,1)} %param.51) | copy-start | bytes 2162692
  115.6 12.0 %all-to-all-start.7 = ((bf16[16,8,1024]{2,1,0:T(8,128)(2,1)}), bf16[16,8,1024]{2,1,0:T(8,128)(2,1)S(1)}, u32[]{:S(2)}, u32[]{:S(2)}) async-start(bf16[16,8,1024]{2,1,0:T(8,128)(2,1)} %tile.2), calls=%async_computation.7 | async-start | bytes 524288 | tf_op jit(solution)/shard_map/all_to_all | solution.py:15
  138.6 9.0 %all-to-all-start.9 = ((bf16[8,128,32]{1,2,0:T(8,128)(2,1)}), bf16[8,128,32]{1,2,0:T(8,128)(2,1)S(1)}, u32[]{:S(2)}, u32[]{:S(2)}) async-start(bf16[8,128,32]{1,2,0:T(8,128)(2,1)} %broadcast_in_dim.28), calls=%async_computation.9 | async-start | bytes 131072 | tf_op jit(solution)/shard_map/all_to_all | solution.py:22
  147.7 31.0 %copy-start.4 = (bf16[1408,256]{1,0:T(8,128)(2,1)S(1)}, bf16[1408,256]{1,0:T(8,128)(2,1)}, u32[]{:S(2)}) copy-start(bf16[1408,256]{1,0:T(8,128)(2,1)} %param.53) | copy-start | bytes 2162692
  149.0 9.8 %all-to-all-start.11 = ((bf16[16,128,1]{1,2,0:T(2,128)(2,1)}), bf16[16,128,1]{1,2,0:T(2,128)(2,1)S(1)}, u32[]{:S(2)}, u32[]{:S(2)}) async-start(bf16[16,128,1]{1,2,0:T(2,128)(2,1)} %transpose.99), calls=%async_computation.11 | async-start | bytes 16384 | tf_op jit(solution)/shard_map/all_to_all | solution.py:49
  152.6 42.4 %copy-start.12 = (bf16[8,3,256]{2,0,1:T(8,128)(2,1)S(1)}, bf16[8,3,256]{2,0,1:T(8,128)(2,1)}, u32[]{:S(2)}) copy-start(bf16[8,3,256]{2,0,1:T(8,128)(2,1)} %param.46) | copy-start | bytes 36868
  152.6 42.3 %copy-start.14 = (bf16[8,3,256]{2,0,1:T(8,128)(2,1)S(1)}, bf16[8,3,256]{2,0,1:T(8,128)(2,1)}, u32[]{:S(2)}) copy-start(bf16[8,3,256]{2,0,1:T(8,128)(2,1)} %param.45) | copy-start | bytes 36868
  158.8 15.4 %all-to-all-start.10 = ((bf16[16,256,88]{1,2,0:T(8,128)(2,1)}), bf16[16,256,88]{1,2,0:T(8,128)(2,1)S(1)}, u32[]{:S(2)}, u32[]{:S(2)}) async-start(bf16[16,256,88]{1,2,0:T(8,128)(2,1)} %bitcast.31), calls=%async_computation.10 | async-start | bytes 1441792 | tf_op jit(solution)/shard_map/all_to_all | solution.py:49
  175.2 11.6 %all-to-all-start.12 = ((bf16[16,128,88]{1,2,0:T(8,128)(2,1)}), bf16[16,128,88]{1,2,0:T(8,128)(2,1)S(1)}, u32[]{:S(2)}, u32[]{:S(2)}) async-start(bf16[16,128,88]{1,2,0:T(8,128)(2,1)} %broadcast_in_dim.29), calls=%async_computation.12 | async-start | bytes 720896 | tf_op jit(solution)/shard_map/all_to_all | solution.py:22
  187.8 12.4 %all-to-all-start.13 = ((f32[8,128,32]{1,2,0:T(8,128)}), f32[8,128,32]{1,2,0:T(8,128)S(1)}, u32[]{:S(2)}, u32[]{:S(2)}) async-start(f32[8,128,32]{1,2,0:T(8,128)} %convolution_bitcast_fusion), calls=%async_computation.13 | async-start | bytes 262144 | tf_op jit(solution)/shard_map/all_to_all | solution.py:43
